TPU v7x, 32 devices: a whole 2x2x4 slice. The times are simulated.
32 devices in a mesh: grp: 2 (over x), ep: 8 (over z, y), tp: 2 (over core).
Axes of the slice: x: 2, y: 2, z: 4, core: 2. Of those that a mesh axis runs over, the one named last changes fastest.
Arguments:
- tokens: bfloat16 [1024, 2048], P(('grp', 'ep')), parts along dimension 0, may hold values from -6 to 6
- routes: int32 [1024, 4], P(('grp', 'ep')), parts along dimension 0, may hold values from 0 to 7, all different within a row; in each aligned block of 64 rows (0 to 63, 64 to 127, ...) at most 64 rows name the same one
- gate_weights: float32 [1024, 4], P(('grp', 'ep')), parts along dimension 0, may hold values from 0.05 to 1
- w_gate: bfloat16 [8, 2048, 1280], P('ep', None, 'tp'), may hold values from -0.125 to 0.125
- w_up: bfloat16 [8, 2048, 1280], P('ep', None, 'tp'), may hold values from -0.125 to 0.125
- w_down: bfloat16 [8, 1280, 2048], P('ep', 'tp'), may hold values from -0.15625 to 0.15625
- norm_gain: float32 [2048], P('tp'), may hold values from 0.1 to 1.9
- norm_bias: float32 [2048], P('tp'), may hold values from -2 to 2
Outputs:
- normed: bfloat16 [1024, 2048], P(('grp', 'ep'), 'tp'), parts along dimension 0
There are 2 independent parts, one for each index of `grp`. A program takes and returns all parts, laid end to end along the dimension named above; an argument that names none is the same for every part. Nothing has to cross between parts.
Inputs may be any that keep to these rules, and one draw needn't show every extreme that they name: `routes`: the rows of a token name distinct experts; in each aligned block of 64 rows (the tokens of one index of ep) no expert is named more than 64 times, a bound that some block reaches.
All inputs are finite; a program needn't handle non-finite values.
Results may differ from a plain program's by a relative error of at most 0.0037.
Values may be sent and summed in bfloat16 or wider, within the bound.
A program may use at most 64 MiB of HBM per device.

v0:
```python
import jax
import jax.numpy as jnp
from jax import lax
from jax.sharding import PartitionSpec as P

residual_scale = 1.4142135
norm_eps = 1e-05


def shards(tokens, routes, gate_weights, w_gate, w_up, w_down, norm_gain, norm_bias):
    num_ep = lax.axis_size("ep")
    num_tp = lax.axis_size("tp")
    tp_index = lax.axis_index("tp")
    tok_rows, width = tokens.shape
    top_count = routes.shape[1]
    experts = num_ep * w_gate.shape[0]
    capacity = 2 * tok_rows * top_count // experts
    half_width = width // num_tp
    pair_list = routes.reshape(-1)
    onehot = (pair_list[:, None] == jnp.arange(experts, dtype=jnp.int32)).astype(jnp.int32)
    slots = jnp.sum((jnp.cumsum(onehot, axis=0) - onehot) * onehot, axis=1)
    target = pair_list * capacity + slots
    placing = jnp.arange(experts * capacity, dtype=jnp.int32)[:, None] == target[None, :]
    placing = jnp.sum(
        placing.reshape(experts * capacity, tok_rows, top_count).astype(jnp.float32), axis=2
    )
    placing = placing.astype(jnp.bfloat16)
    own_half = lax.dynamic_slice_in_dim(tokens, tp_index * half_width, half_width, 1)
    outgoing = jnp.dot(placing, own_half, preferred_element_type=jnp.float32).astype(jnp.bfloat16)
    arrived = lax.all_to_all(outgoing, "ep", split_axis=0, concat_axis=0, tiled=True)
    received = lax.all_gather(arrived, "tp", axis=1, tiled=True)
    gate = jnp.dot(received, w_gate[0], preferred_element_type=jnp.float32)
    upper = jnp.dot(received, w_up[0], preferred_element_type=jnp.float32)
    hidden = (jax.nn.silu(gate) * upper).astype(jnp.bfloat16)
    partial_sum = jnp.dot(hidden, w_down[0], preferred_element_type=jnp.float32).astype(
        jnp.bfloat16
    )
    expert_out = (
        lax.psum_scatter(partial_sum, "tp", scatter_dimension=1, tiled=True)
        .astype(jnp.float32)
        .astype(jnp.bfloat16)
    )
    came_back = lax.all_to_all(expert_out, "ep", split_axis=0, concat_axis=0, tiled=True)
    chosen = came_back[target].astype(jnp.float32).reshape(tok_rows, top_count, half_width)
    mixture = jnp.sum(gate_weights[:, :, None] * chosen, axis=1).astype(jnp.bfloat16)
    own_tokens = lax.dynamic_slice_in_dim(tokens, tp_index * half_width, half_width, 1)
    summed = residual_scale * own_tokens.astype(jnp.float32) + mixture.astype(jnp.float32)
    row_sum, row_squares = lax.psum(
        (jnp.sum(summed, axis=1), jnp.sum(summed * summed, axis=1)), "tp"
    )
    mean = row_sum / width
    variance = row_squares / width - mean * mean
    normed = (summed - mean[:, None]) * lax.rsqrt(
        variance[:, None] + norm_eps
    ) * norm_gain + norm_bias
    return normed.astype(jnp.bfloat16)


def solution(mesh):
    in_specs = (
        P(("grp", "ep"), None),
        P(("grp", "ep"), None),
        P(("grp", "ep"), None),
        P("ep", None, "tp"),
        P("ep", None, "tp"),
        P("ep", "tp", None),
        P("tp"),
        P("tp"),
    )
    out_specs = P(("grp", "ep"), "tp")
    return jax.shard_map(shards, mesh=mesh, in_specs=in_specs, out_specs=out_specs, check_vma=False)
```

profile of v0, /device:TPU:0, one launch (start us, length us, event | category | flops | bytes accessed | tf_op | source)
XLA Modules:
  0.0 125.9 jit_solution(16409182615999726836)
XLA Ops:
  6.5 0.9 copy.16
  7.5 0.1 eq.44
  7.6 0.1 eq.40
  7.7 0.6 reduce-window.6
  8.3 0.2 slice_reduce_fusion
  8.5 0.1 fusion.18
  8.6 0.1 reduce_sum.50
  8.8 0.1 convert_reduce_fusion
  9.0 1.4 %convolution_convert_fusion.1 = bf16[512,1024]{1,0:T(8,128)(2,1)S(1)} fusion(bf16[64,2048]{1,0:T(8,128)(2,1)} %param.8, s32[]{:T(128)S(6)} %select_n.14, bf16[512,64]{0,1:T(8,128)(2,1)S(1)} %convert_reduce_fusion), kind=kOutput, calls=%fused_computation.7 | convolution fusion | flops 67633152 | bytes 1245188 | tf_op jit(solution)/shard_map/dot_general | solution.py:29
  10.3 33.0 %all_to_all.24 = bf16[8,64,1024]{2,1,0:T(8,128)(2,1)} all-to-all(bf16[8,64,1024]{2,1,0:T(8,128)(2,1)S(1)} %bitcast.33), channel_id=1, replica_groups=mesh['grp'=2,'ep'=8,'tp'=2] {'ep'}, dimensions={0} | all-to-all | bytes 2097152 | tf_op jit(solution)/shard_map/all_to_all | solution.py:30
  43.4 9.7 %all-gather.2.cloned.1.call-done = bf16[512,2048]{1,0:T(8,128)(2,1)} async-done(((bf16[512,1024]{1,0:T(8,128)(2,1)}), bf16[512,2048]{1,0:T(8,128)(2,1)}) %all-gather.2.cloned.1.call-update) | async-done | bytes 2097168 | tf_op jit(solution)/shard_map/all_gather | solution.py:31
  53.1 5.2 %fusion.3 = f32[512,640]{1,0:T(8,128)} fusion(bf16[512,2048]{1,0:T(8,128)(2,1)} %all-gather.2.cloned.1.call-done, bf16[1,2048,640]{2,1,0:T(8,128)(2,1)} %param.11), kind=kOutput, calls=%fused_computation.5 | convolution fusion | flops 1342177280 | bytes 6029312 | tf_op jit(solution)/shard_map/dot_general | solution.py:32
  58.3 8.0 %convolution_convert_fusion = bf16[512,2048]{1,0:T(8,128)(2,1)} fusion(bf16[1,640,2048]{2,1,0:T(8,128)(2,1)S(1)} %copy-done, bf16[512,2048]{1,0:T(8,128)(2,1)} %all-gather.2.cloned.1.call-done, bf16[1,2048,640]{2,1,0:T(8,128)(2,1)} %param.12, f32[512,640]{1,0:T(8,128)} %fusion.3), kind=kOutput, calls=%fused_computation.1 | convolution fusion | flops 2687369216 | bytes 10747904 | tf_op jit(solution)/shard_map/dot_general | solution.py:35
  66.3 11.0 %reduce-scatter.2.cloned.1.call-done = bf16[512,1024]{1,0:T(8,128)(2,1)} async-done(((bf16[512,2048]{1,0:T(8,128)(2,1)}), bf16[512,1024]{1,0:T(8,128)(2,1)}) %reduce-scatter.2.cloned.1.call-update) | async-done | bytes 1048592 | tf_op jit(solution)/shard_map/reduce_scatter | solution.py:39
  77.3 5.9 %all-to-all-start.1 = ((bf16[8,64,1024]{2,1,0:T(8,128)(2,1)}), bf16[8,64,1024]{2,1,0:T(8,128)(2,1)}, u32[]{:S(2)}, u32[]{:S(2)}) async-start(bf16[8,64,1024]{2,1,0:T(8,128)(2,1)} %bitcast.34), calls=%async_computation.2 | async-start | bytes 2097152 | tf_op jit(solution)/shard_map/all_to_all | solution.py:43
  83.1 0.1 mul.79
  83.2 0.1 copy.15
  83.3 26.0 %all-to-all-done.1 = bf16[8,64,1024]{2,1,0:T(8,128)(2,1)} async-done(((bf16[8,64,1024]{2,1,0:T(8,128)(2,1)}), bf16[8,64,1024]{2,1,0:T(8,128)(2,1)}, u32[]{:S(2)}, u32[]{:S(2)}) %all-to-all-start.1) | async-done | bytes 1048608 | tf_op jit(solution)/shard_map/all_to_all | solution.py:43
  109.3 2.9 %gather_fusion = bf16[256,1024]{1,0:T(8,128)(2,1)S(1)} fusion(bf16[512,1024]{1,0:T(8,128)(2,1)} %bitcast.8, s32[1024]{0:T(1024)S(1)} %pad_clamp_fusion), kind=kCustom, calls=%fused_computation | custom fusion | bytes 1049600 | tf_op jit(solution)/shard_map/gather | solution.py:44
  112.3 1.3 %reshape.79 = f32[64,4,1024]{2,1,0:T(4,128)} reshape(bf16[256,1024]{1,0:T(8,128)(2,1)S(1)} %gather_fusion) | data formatting | bytes 1572864 | tf_op jit(solution)/shard_map/convert_element_type | solution.py:44
  113.6 2.0 %multiply_reduce_fusion = bf16[64,1024]{1,0:T(8,128)(2,1)S(1)} fusion(f32[64,4,1024]{2,1,0:T(4,128)} %reshape.79, f32[64,4]{1,0:T(8,128)S(1)} %copy.15), kind=kLoop, calls=%fused_computation.10 | loop fusion | flops 458752 | bytes 1180672 | tf_op jit(solution)/shard_map/reduce_sum | solution.py:45
  115.6 0.2 fusion.14
  115.8 2.5 %all-reduce = (f32[64]{0:T(128)S(1)}, f32[64]{0:T(128)S(1)}) all-reduce(f32[64]{0:T(128)S(1)} %get-tuple-element.6, f32[64]{0:T(128)S(1)} %get-tuple-element.5), channel_id=1, replica_groups=mesh['grp'=2,'ep'=8,'tp'=2] {'tp'}, use_global_device_ids=true, to_apply=%region_9.10 | all-reduce | flops 128 | bytes 1024 | tf_op jit(solution)/shard_map/psum | solution.py:48
  118.3 0.8 add_convert_fusion
  (22 shorter events, 0.3 us)
Async XLA Ops:
  6.5 51.8 %copy-start = (bf16[1,640,2048]{2,1,0:T(8,128)(2,1)S(1)}, bf16[1,640,2048]{2,1,0:T(8,128)(2,1)}, u32[]{:S(2)}) copy-start(bf16[1,640,2048]{2,1,0:T(8,128)(2,1)} %param.13) | copy-start | bytes 7864324
  6.5 46.5 %all-gather.2.cloned.1.call-start = ((), (), s32[]{:S(2)}) async-start(), calls=%async_computation.3 | async-start | bytes 3145728 | tf_op jit(solution)/shard_map/all_gather | solution.py:31
  43.3 33.9 %reduce-scatter.2.cloned.1.call-start = ((), (), s32[]{:S(2)}) async-start(), calls=%async_computation.4 | async-start | bytes 3145728 | tf_op jit(solution)/shard_map/reduce_scatter | solution.py:39
  66.3 17.0 %copy-start.4 = (f32[64,4]{0,1:T(4,128)S(1)}, f32[64,4]{0,1:T(4,128)}, u32[]{:S(2)}) copy-start(f32[64,4]{0,1:T(4,128)} %param.10) | copy-start | bytes 3076
  77.3 32.1 %all-to-all-start.1 = ((bf16[8,64,1024]{2,1,0:T(8,128)(2,1)}), bf16[8,64,1024]{2,1,0:T(8,128)(2,1)}, u32[]{:S(2)}, u32[]{:S(2)}) async-start(bf16[8,64,1024]{2,1,0:T(8,128)(2,1)} %bitcast.34), calls=%async_computation.2 | async-start | bytes 2097152 | tf_op jit(solution)/shard_map/all_to_all | solution.py:43
  112.3 3.3 %copy-start.1 = (bf16[64,2048]{1,0:T(8,128)(2,1)S(1)}, bf16[64,2048]{1,0:T(8,128)(2,1)}, u32[]{:S(2)}) copy-start(bf16[64,2048]{1,0:T(8,128)(2,1)} %param.8) | copy-start | bytes 786436
  112.3 6.0 %copy-start.2 = (f32[1024]{0:T(1024)S(1)}, f32[1024]{0:T(1024)}, u32[]{:S(2)}) copy-start(f32[1024]{0:T(1024)} %param.15) | copy-start | bytes 12292
  112.3 6.0 %copy-start.3 = (f32[1024]{0:T(1024)S(1)}, f32[1024]{0:T(1024)}, u32[]{:S(2)}) copy-start(f32[1024]{0:T(1024)} %param.14) | copy-start | bytes 12292
Sparse Core Ops, SparseCore 0:
  43.5 9.5 all-gather.1
  66.4 10.7 reduce-scatter.1
where the time goes:
time: 126 us
  waiting for transfers between devices  46.7 us (37%)
  blocking collectives  35.4 us (28%)
  matrix products  14.6 us (12%)
  between operations  13.5 us (11%)
  local copies, waits for them, and re-layouts  5.99 us (5%)
  starting transfers between devices  5.91 us (5%)
  other arithmetic  3.78 us (3%)
    all_to_all x1, blocking collectives, shards(): lax.all_to_all(outgoing, 'ep', split_axis=0, concat_axis=0, tiled=True)  33 us
    all_to_all x1, waiting for transfers between devices, shards(): lax.all_to_all(expert_out, 'ep', split_axis=0, concat_axis=0, tiled=True)  26 us
    reduce_scatter x1, waiting for transfers between devices, shards(): lax.psum_scatter(partial_sum, 'tp', scatter_dimension=1, tiled=True)  11 us
    all_gather x1, waiting for transfers between devices, shards(): received = lax.all_gather(arrived, 'tp', axis=1, tiled=True)  9.68 us
    dot_general x1, matrix products, shards(): jnp.dot(hidden, w_down[0], preferred_element_type=jnp.float32)  7.98 us
    all_to_all x1, starting transfers between devices, shards(): lax.all_to_all(expert_out, 'ep', split_axis=0, concat_axis=0, tiled=True)  5.87 us
    dot_general x1, matrix products, shards(): gate = jnp.dot(received, w_gate[0], preferred_element_type=jnp.float32)  5.21 us
    gather x1, local copies, waits for them, and re-layouts, shards(): came_back[target].astype(jnp.float32)  2.92 us
  transfers between devices with their start and end apart: 3, of which 3 were waited for; matrix products, arithmetic and copies ran while one was open for 0% of the time, Pallas kernels for 0%

commit v1 on v0

v1 whole, which is shorter than its diff:
```python
import functools
import jax
import jax.numpy as jnp
from jax import lax
from jax.experimental import pallas as pl
from jax.experimental.pallas import tpu as pltpu
from jax.sharding import PartitionSpec as P

residual_scale = 1.4142135
norm_eps = 1e-05
MESH = pl.DeviceIdType.MESH
LANES = 128


def kernel(n, num_tp, tokens, routes, weights, gain, bias, wg_hbm, wu_hbm, wd_hbm, out,
           xs, wg, wu, wd, own, part_out, part_in, ret_out, ret_in, stat_out, stat_in,
           w_sem, gs, gr, fs, fr, ps, pr, rs, rr, ss, sr):
    me = lax.axis_index("ep")
    core = lax.axis_index("tp")
    other = lax.rem(core + 1, num_tp)
    rows, width = tokens.shape
    half = width // num_tp
    share = rows // num_tp
    pairs = n // 2
    z, y = me // 2, lax.rem(me, 2)
    partner = 2 * z + 1 - y
    my_rows = pl.ds(pl.multiple_of(core * share, share), share)
    my_cols = pl.ds(pl.multiple_of(core * half, half), half)
    other_cols = pl.ds(pl.multiple_of(other * half, half), half)

    loads = [pltpu.make_async_copy(a.at[0], b, w_sem.at[i])
             for i, (a, b) in enumerate(((wg_hbm, wg), (wu_hbm, wu), (wd_hbm, wd)))]
    for load in loads:
        load.start()

    barrier = pltpu.get_barrier_semaphore()
    for k in range(1, n):
        pl.semaphore_signal(barrier, inc=1, device_id={"ep": lax.rem(me + k, n)}, device_id_type=MESH)
    pl.semaphore_signal(barrier, inc=1, device_id={"tp": other}, device_id_type=MESH)
    xs[me] = tokens[...]
    pl.semaphore_wait(barrier, n)

    def offset(g):
        step = (g + 1) // 2
        return step * (2 * lax.rem(g, 2) - 1)

    def ahead(g):
        return lax.rem(z + offset(g) + pairs, pairs)

    def behind(g):
        return lax.rem(z - offset(g) + pairs, pairs)

    def gather_copy(target, source):
        return pltpu.make_async_remote_copy(
            src_ref=tokens.at[my_rows, :], dst_ref=xs.at[source, my_rows, :],
            send_sem=gs.at[target], recv_sem=gr.at[source],
            device_id={"ep": target}, device_id_type=MESH)

    def forward_copy(source, who):
        part = pl.ds(pl.multiple_of(who * share, share), share)
        return pltpu.make_async_remote_copy(
            src_ref=xs.at[source, part, :], dst_ref=xs.at[source, part, :],
            send_sem=fs.at[source], recv_sem=fr.at[source],
            device_id={"tp": other}, device_id_type=MESH)

    def partial_copy(zz):
        block = pl.ds(2 * zz, 2)
        return pltpu.make_async_remote_copy(
            src_ref=part_out.at[block], dst_ref=part_in.at[block],
            send_sem=ps.at[zz], recv_sem=pr.at[zz],
            device_id={"tp": other}, device_id_type=MESH)

    def return_copy(target, source):
        return pltpu.make_async_remote_copy(
            src_ref=ret_out.at[target], dst_ref=ret_in.at[source],
            send_sem=rs.at[target], recv_sem=rr.at[source],
            device_id={"ep": target}, device_id_type=MESH)

    gather_copy(partner, me).start()

    def send_tokens(g, carry):
        zz = behind(g)
        gather_copy(2 * zz + y, me).start()
        gather_copy(2 * zz + 1 - y, me).start()
        return carry

    lax.fori_loop(1, pairs, send_tokens, 0)

    def pass_on(source):
        gather_copy(partner, source).wait_recv()
        forward_copy(source, core).start()

    def finish(g):
        zz = ahead(g)
        partial_copy(zz).wait_recv()
        block = pl.ds(2 * zz, 2)
        total = own[block] + part_in[block].astype(jnp.float32)
        ret_out[block] = total.astype(jnp.bfloat16)

    def step(i, carry):
        @pl.when(i == 0)
        def _():
            pass_on(partner)

        @pl.when((i > 0) & (i < pairs))
        def _():
            zz = ahead(i)
            pass_on(2 * zz + y)
            pass_on(2 * zz + 1 - y)

        @pl.when(i == 1)
        def _():
            for load in loads:
                load.wait()
            forward_copy(partner, other).wait_recv()

        @pl.when((i > 1) & (i <= pairs))
        def _():
            zz = ahead(i - 1)
            forward_copy(2 * zz, other).wait_recv()
            forward_copy(2 * zz + 1, other).wait_recv()

        @pl.when((i > 0) & (i <= pairs))
        def _():
            zz = ahead(i - 1)
            block = pl.ds(2 * zz, 2)
            x = xs[block].reshape(2 * rows, width)
            gate = jnp.dot(x, wg[...], preferred_element_type=jnp.float32)
            upper = jnp.dot(x, wu[...], preferred_element_type=jnp.float32)
            hidden = (gate / (1.0 + jnp.exp(-gate)) * upper).astype(jnp.bfloat16)
            theirs = jnp.dot(hidden, wd[:, other_cols], preferred_element_type=jnp.float32)
            part_out[block] = theirs.astype(jnp.bfloat16).reshape(2, rows, half)
            partial_copy(zz).start()
            mine = jnp.dot(hidden, wd[:, my_cols], preferred_element_type=jnp.float32)
            own[block] = mine.reshape(2, rows, half)

        @pl.when(i == 2)
        def _():
            finish(0)
            return_copy(partner, me).start()

        @pl.when(i > 2)
        def _():
            finish(i - 2)
            zz = ahead(i - 2)
            return_copy(2 * zz + y, me).start()
            return_copy(2 * zz + 1 - y, me).start()

        return carry

    lax.fori_loop(0, pairs + 2, step, 0)

    route = routes[...]
    weight = weights[...]

    def weighted(source, block):
        w = jnp.sum(jnp.where(route == source, weight, 0.0), axis=1, keepdims=True)
        return w * block.astype(jnp.float32)

    return_copy(partner, partner).wait_recv()
    own[0] = weighted(me, ret_out[me]) + weighted(partner, ret_in[partner])

    def collect(g, carry):
        zz = behind(g)
        return_copy(partner, 2 * zz + y).wait_recv()
        return_copy(partner, 2 * zz + 1 - y).wait_recv()
        own[0] = own[0] + weighted(2 * zz, ret_in[2 * zz]) + weighted(2 * zz + 1, ret_in[2 * zz + 1])
        return carry

    lax.fori_loop(1, pairs, collect, 0)
    mixture = own[0].astype(jnp.bfloat16).astype(jnp.float32)
    summed = residual_scale * tokens[:, my_cols].astype(jnp.float32) + mixture
    row_sum = jnp.sum(summed, axis=1, keepdims=True)
    row_squares = jnp.sum(summed * summed, axis=1, keepdims=True)
    lane = lax.broadcasted_iota(jnp.int32, (rows, LANES), 1)
    stat_out[...] = jnp.where(lane == 0, row_sum, row_squares)
    stats = pltpu.make_async_remote_copy(
        src_ref=stat_out, dst_ref=stat_in, send_sem=ss, recv_sem=sr,
        device_id={"tp": other}, device_id_type=MESH)
    stats.start()

    gather_copy(partner, me).wait_send()
    forward_copy(partner, core).wait_send()
    partial_copy(z).wait_send()
    return_copy(partner, me).wait_send()

    def drain(g, carry):
        zz = ahead(g)
        partial_copy(zz).wait_send()
        for j in range(2):
            gather_copy(2 * zz + j, me).wait_send()
            forward_copy(2 * zz + j, core).wait_send()
            return_copy(2 * zz + j, me).wait_send()
        return carry

    lax.fori_loop(1, pairs, drain, 0)
    stats.wait()
    row_sum = row_sum + stat_in[:, 0:1]
    row_squares = row_squares + stat_in[:, 1:2]
    mean = row_sum / width
    variance = row_squares / width - mean * mean
    normed = (summed - mean) * lax.rsqrt(variance + norm_eps) * gain[...] + bias[...]
    out[...] = normed.astype(jnp.bfloat16)


def shards(n, num_tp, tokens, routes, gate_weights, w_gate, w_up, w_down, norm_gain, norm_bias):
    rows, width = tokens.shape
    hidden = w_gate.shape[2]
    half = width // num_tp
    vmem = pl.BlockSpec(memory_space=pltpu.VMEM)
    hbm = pl.BlockSpec(memory_space=pl.ANY)
    dma = pltpu.SemaphoreType.DMA
    return pl.pallas_call(
        functools.partial(kernel, n, num_tp),
        out_shape=jax.ShapeDtypeStruct((rows, half), jnp.bfloat16),
        in_specs=[vmem] * 5 + [hbm] * 3,
        out_specs=vmem,
        scratch_shapes=[
            pltpu.VMEM((n, rows, width), jnp.bfloat16),
            pltpu.VMEM((width, hidden), jnp.bfloat16),
            pltpu.VMEM((width, hidden), jnp.bfloat16),
            pltpu.VMEM((hidden, width), jnp.bfloat16),
            pltpu.VMEM((n, rows, half), jnp.float32),
            pltpu.VMEM((n, rows, half), jnp.bfloat16),
            pltpu.VMEM((n, rows, half), jnp.bfloat16),
            pltpu.VMEM((n, rows, half), jnp.bfloat16),
            pltpu.VMEM((n, rows, half), jnp.bfloat16),
            pltpu.VMEM((rows, LANES), jnp.float32),
            pltpu.VMEM((rows, LANES), jnp.float32),
            dma((3,)), dma((n,)), dma((n,)), dma((n,)), dma((n,)), dma((n // 2,)), dma((n // 2,)),
            dma((n,)), dma((n,)), dma, dma,
        ],
        compiler_params=pltpu.CompilerParams(collective_id=0, has_side_effects=True),
    )(tokens, routes, gate_weights, norm_gain.reshape(1, half), norm_bias.reshape(1, half),
      w_gate, w_up, w_down)


def solution(mesh):
    in_specs = (
        P(("grp", "ep"), None),
        P(("grp", "ep"), None),
        P(("grp", "ep"), None),
        P("ep", None, "tp"),
        P("ep", None, "tp"),
        P("ep", "tp", None),
        P("tp"),
        P("tp"),
    )
    out_specs = P(("grp", "ep"), "tp")
    body = functools.partial(shards, mesh.shape["ep"], mesh.shape["tp"])
    return jax.shard_map(body, mesh=mesh, in_specs=in_specs, out_specs=out_specs, check_vma=False)
```

time: 126 us -> 61.7 us (0.49)
  Pallas kernels: 0 us -> 57.2 us
  waiting for transfers between devices: 46.7 us -> 0 us
  blocking collectives: 35.4 us -> 0 us
  matrix products: 14.6 us -> 0 us
  between operations: 13.5 us -> 0.01 us
  starting transfers between devices: 5.91 us -> 0 us
  other arithmetic: 3.78 us -> 0 us
  local copies, waits for them, and re-layouts: 5.99 us -> 4.32 us
    pallas_call x0 -> x1, Pallas kernels: none -> 57.2 us  [shards(): pl.pallas_call(functools.partial(kernel, n, num_tp), out_shape=jax.ShapeD...]
    all_to_all x1 -> x0, blocking collectives: 33 us -> none  [shards(): lax.all_to_all(outgoing, 'ep', split_axis=0, concat_axis=0, tiled=True)]
    all_to_all x1 -> x0, waiting for transfers between devices: 26 us -> none  [shards(): lax.all_to_all(expert_out, 'ep', split_axis=0, concat_axis=0, tiled=True)]
    dot_general x3 -> x0, matrix products: 14.6 us -> none  [the longest x1 7.98 us: shards(): jnp.dot(hidden, w_down[0], preferred_element_type=jnp.float32)]
    reduce_scatter x1 -> x0, waiting for transfers between devices: 11 us -> none  [shards(): lax.psum_scatter(partial_sum, 'tp', scatter_dimension=1, tiled=True)]
    all_gather x1 -> x0, waiting for transfers between devices: 9.68 us -> none  [shards(): received = lax.all_gather(arrived, 'tp', axis=1, tiled=True)]
    all_to_all x1 -> x0, starting transfers between devices: 5.87 us -> none  [shards(): lax.all_to_all(expert_out, 'ep', split_axis=0, concat_axis=0, tiled=True)]
    unnamed x12 -> x3, local copies, waits for them, and re-layouts: 1.04 us -> 4.32 us
  transfers between devices with their start and end apart: 3 -> 0, of which waited for: 3 -> 0; matrix products, arithmetic and copies ran while one was open for 0% -> 0% of each run, Pallas kernels for 0% -> 0%
where the time goes in v1:
time: 61.7 us; the launch traced here: 61.5 us
  Pallas kernels  57.2 us (93%)
  local copies, waits for them, and re-layouts  4.32 us (7%)
    pallas_call x1, Pallas kernels, shards(): pl.pallas_call(functools.partial(kernel, n, num_tp), out_shape=jax.ShapeD...  57.2 us
    unnamed x3, local copies, waits for them, and re-layouts  4.32 us

profile of v1, /device:TPU:0, one launch (start us, length us, event | category | flops | bytes accessed | tf_op | source)
XLA Modules:
  0.0 61.5 jit_solution(8409501272386898646)
XLA Ops:
  0.0 1.4 %copy.9.routes = s32[64,4]{1,0:T(8,128)} copy(s32[64,4]{0,1:T(4,128)} %param.9) | data formatting | bytes 2048 | tf_op args[1]
  1.4 1.4 %copy.10.weights = f32[64,4]{1,0:T(8,128)} copy(f32[64,4]{0,1:T(4,128)} %param.10) | data formatting | bytes 2048 | tf_op args[2]
  2.8 57.2 %shard_map.82 = bf16[64,1024]{1,0:T(8,128)(2,1)} custom-call(bf16[64,2048]{1,0:T(8,128)(2,1)} %tokens.1, s32[64,4]{1,0:T(8,128)} %copy.9.routes, f32[64,4]{1,0:T(8,128)} %copy.10.weights, f32[1,1024]{1,0:T(1,128)} %bitcast.2, f32[1,1024]{1,0:T(1,128)} %bitcast.3, bf16[1,2048,640]{2,1,0:T(8,128)(2,1)} %wg_hbm.1, bf16[1,2048,640]{2,1,0:T(8,128)(2,1)} %wu_hbm.1, ...), custom_call_target="tpu_custom_call" | custom-call | tf_op jit(solution)/shard_map/pallas_call | solution.py:213
  59.9 1.6 %copy.12 = bf16[64,1024]{1,0:T(8,128)(2,1)} copy(bf16[64,1024]{1,0:T(8,128)(2,1)} %shard_map.82) | data formatting | bytes 262144

commit v2 on v1

v2 whole, which is shorter than its diff:
```python
import functools
import jax
import jax.numpy as jnp
from jax import lax
from jax.experimental import pallas as pl
from jax.experimental.pallas import tpu as pltpu
from jax.sharding import PartitionSpec as P

residual_scale = 1.4142135
norm_eps = 1e-05
MESH = pl.DeviceIdType.MESH
LANES = 128


def kernel(n, num_tp, tokens, routes, weights, gain, bias, wg_hbm, wu_hbm, wd_hbm, out,
           xs, wg, wu, wd, own, part_out, part_in, y_out, y_in, ret_out, ret_in,
           table_out, table_in, stat_out, stat_in,
           w_sem, gs, gr, ys, yr, fs, fr, ps, pr, vs, vr, rs, rr, ts, tr, ss, sr):
    me = lax.axis_index("ep")
    core = lax.axis_index("tp")
    other = lax.rem(core + 1, num_tp)
    rows, width = tokens.shape
    half = width // num_tp
    share = rows // num_tp
    pairs = n // 2
    z, y = me // 2, lax.rem(me, 2)
    partner = 2 * z + 1 - y
    my_rows = pl.ds(pl.multiple_of(core * share, share), share)
    my_cols = pl.ds(pl.multiple_of(core * half, half), half)
    other_cols = pl.ds(pl.multiple_of(other * half, half), half)

    loads = [pltpu.make_async_copy(a.at[0], b, w_sem.at[i])
             for i, (a, b) in enumerate(((wg_hbm, wg), (wu_hbm, wu), (wd_hbm, wd)))]
    for load in loads:
        load.start()

    barrier = pltpu.get_barrier_semaphore()
    for k in range(1, n):
        pl.semaphore_signal(barrier, inc=1, device_id={"ep": lax.rem(me + k, n)}, device_id_type=MESH)
    pl.semaphore_signal(barrier, inc=1, device_id={"tp": other}, device_id_type=MESH)
    xs[me] = tokens[...]
    expert = lax.broadcasted_iota(jnp.int32, (n, rows), 0)
    table = jnp.zeros((n, rows), jnp.float32)
    for k in range(routes.shape[0]):
        table = table + jnp.where(routes[k:k + 1, :] == expert, weights[k:k + 1, :], 0.0)
    table_out[...] = table
    table_in[me] = table
    pl.semaphore_wait(barrier, n)

    def mate(g):
        total = 0
        bit = 1
        while bit < pairs:
            total = total + bit * lax.rem(z // bit + g // bit, 2)
            bit *= 2
        return total

    def own_copy():
        return pltpu.make_async_remote_copy(
            src_ref=tokens.at[my_rows, :], dst_ref=xs.at[me, my_rows, :],
            send_sem=ys.at[z], recv_sem=yr.at[z],
            device_id={"ep": partner}, device_id_type=MESH)

    def gather_copy(there, source):
        return pltpu.make_async_remote_copy(
            src_ref=tokens.at[my_rows, :], dst_ref=xs.at[2 * source + y, my_rows, :],
            send_sem=gs.at[there], recv_sem=gr.at[source],
            device_id={"ep": 2 * there + y}, device_id_type=MESH)

    def across_copy(zz, side):
        return pltpu.make_async_remote_copy(
            src_ref=xs.at[2 * zz + side, my_rows, :], dst_ref=xs.at[2 * zz + side, my_rows, :],
            send_sem=ys.at[zz], recv_sem=yr.at[zz],
            device_id={"ep": partner}, device_id_type=MESH)

    def forward_copy(source, who):
        part = pl.ds(pl.multiple_of(who * share, share), share)
        return pltpu.make_async_remote_copy(
            src_ref=xs.at[source, part, :], dst_ref=xs.at[source, part, :],
            send_sem=fs.at[source], recv_sem=fr.at[source],
            device_id={"tp": other}, device_id_type=MESH)

    def partial_copy(zz):
        block = pl.ds(2 * zz, 2)
        return pltpu.make_async_remote_copy(
            src_ref=part_out.at[block], dst_ref=part_in.at[block],
            send_sem=ps.at[zz], recv_sem=pr.at[zz],
            device_id={"tp": other}, device_id_type=MESH)

    def back_copy(zz):
        return pltpu.make_async_remote_copy(
            src_ref=y_out.at[zz], dst_ref=y_in.at[zz],
            send_sem=vs.at[zz], recv_sem=vr.at[zz],
            device_id={"ep": partner}, device_id_type=MESH)

    def return_copy(there, source):
        return pltpu.make_async_remote_copy(
            src_ref=ret_out.at[there], dst_ref=ret_in.at[source],
            send_sem=rs.at[there], recv_sem=rr.at[source],
            device_id={"ep": 2 * there + y}, device_id_type=MESH)

    def table_copy(there, source):
        return pltpu.make_async_remote_copy(
            src_ref=table_out, dst_ref=table_in.at[source],
            send_sem=ts.at[there], recv_sem=tr.at[source],
            device_id={"ep": there}, device_id_type=MESH)

    own_copy().start()
    for g in range(1, pairs):
        gather_copy(mate(g), z).start()
    for k in range(1, n):
        table_copy(lax.rem(me + k, n), me).start()

    diagonal = (lax.broadcasted_iota(jnp.int32, (rows, rows), 0)
                == lax.broadcasted_iota(jnp.int32, (rows, rows), 1))

    def weight_of(source):
        row = table_in[source, pl.ds(me, 1), :]
        return jnp.sum(jnp.where(diagonal, row, 0.0), axis=1, keepdims=True)

    def step(i, carry):
        @pl.when((i > 0) & (i < pairs))
        def _():
            zz = mate(i)
            gather_copy(zz, zz).wait_recv()
            across_copy(zz, y).start()
            forward_copy(2 * zz + y, core).start()

        @pl.when((i > 0) & (i <= pairs))
        def _():
            zz = mate(i - 1)
            across_copy(zz, 1 - y).wait_recv()
            forward_copy(2 * zz + 1 - y, core).start()

        @pl.when(i == 2)
        def _():
            for load in loads:
                load.wait()
            forward_copy(partner, other).wait_recv()

        @pl.when((i > 2) & (i <= pairs + 1))
        def _():
            zz = mate(i - 2)
            forward_copy(2 * zz, other).wait_recv()
            forward_copy(2 * zz + 1, other).wait_recv()

        @pl.when((i > 1) & (i <= pairs + 1))
        def _():
            zz = mate(i - 2)
            block = pl.ds(2 * zz, 2)
            x = xs[block].reshape(2 * rows, width)
            gate = jnp.dot(x, wg[...], preferred_element_type=jnp.float32)
            upper = jnp.dot(x, wu[...], preferred_element_type=jnp.float32)
            hidden = (gate / (1.0 + jnp.exp(-gate)) * upper).astype(jnp.bfloat16)
            theirs = jnp.dot(hidden, wd[:, other_cols], preferred_element_type=jnp.float32)
            part_out[block] = theirs.astype(jnp.bfloat16).reshape(2, rows, half)
            partial_copy(zz).start()
            mine = jnp.dot(hidden, wd[:, my_cols], preferred_element_type=jnp.float32)
            own[block] = mine.reshape(2, rows, half)

        @pl.when(i == 3)
        def _():
            table_copy(partner, partner).wait_recv()

        @pl.when((i > 3) & (i <= pairs + 2))
        def _():
            zz = mate(i - 3)
            table_copy(partner, 2 * zz).wait_recv()
            table_copy(partner, 2 * zz + 1).wait_recv()

        @pl.when((i > 2) & (i <= pairs + 2))
        def _():
            zz = mate(i - 3)
            partial_copy(zz).wait_recv()
            away = 2 * zz + 1 - y
            total = own[away] + part_in[away].astype(jnp.float32)
            y_out[zz] = (total * weight_of(away)).astype(jnp.bfloat16)
            back_copy(zz).start()
            here = 2 * zz + y
            total = own[here] + part_in[here].astype(jnp.float32)
            own[here] = total * weight_of(here)

        @pl.when(i > 3)
        def _():
            zz = mate(i - 4)
            here = 2 * zz + y
            back_copy(zz).wait_recv()
            total = own[here] + y_in[zz].astype(jnp.float32)
            own[here] = total
            ret_out[zz] = total.astype(jnp.bfloat16)

        @pl.when(i > 4)
        def _():
            return_copy(mate(i - 4), z).start()

        return carry

    lax.fori_loop(0, pairs + 4, step, 0)

    def collect(g, total):
        zz = mate(g)
        return_copy(zz, zz).wait_recv()
        return total + ret_in[zz].astype(jnp.float32)

    mixture = own[me]
    for g in range(1, pairs):
        mixture = collect(g, mixture)
    mixture = mixture.astype(jnp.bfloat16).astype(jnp.float32)
    summed = residual_scale * tokens[:, my_cols].astype(jnp.float32) + mixture
    row_sum = jnp.sum(summed, axis=1, keepdims=True)
    row_squares = jnp.sum(summed * summed, axis=1, keepdims=True)
    lane = lax.broadcasted_iota(jnp.int32, (rows, LANES), 1)
    stat_out[...] = jnp.where(lane == 0, row_sum, row_squares)
    stats = pltpu.make_async_remote_copy(
        src_ref=stat_out, dst_ref=stat_in, send_sem=ss, recv_sem=sr,
        device_id={"tp": other}, device_id_type=MESH)
    stats.start()

    own_copy().wait_send()
    forward_copy(partner, core).wait_send()
    partial_copy(z).wait_send()
    back_copy(z).wait_send()
    table_copy(partner, me).wait_send()

    def drain(g, carry):
        zz = mate(g)
        gather_copy(zz, z).wait_send()
        across_copy(zz, y).wait_send()
        partial_copy(zz).wait_send()
        back_copy(zz).wait_send()
        return_copy(zz, z).wait_send()
        for j in range(2):
            forward_copy(2 * zz + j, core).wait_send()
            table_copy(2 * zz + j, me).wait_send()
        return carry

    lax.fori_loop(1, pairs, drain, 0)
    stats.wait()
    row_sum = row_sum + stat_in[:, 0:1]
    row_squares = row_squares + stat_in[:, 1:2]
    mean = row_sum / width
    variance = row_squares / width - mean * mean
    normed = (summed - mean) * lax.rsqrt(variance + norm_eps) * gain[...] + bias[...]
    out[...] = normed.astype(jnp.bfloat16)


def shards(n, num_tp, tokens, routes, gate_weights, w_gate, w_up, w_down, norm_gain, norm_bias):
    rows, width = tokens.shape
    hidden = w_gate.shape[2]
    half = width // num_tp
    pairs = n // 2
    vmem = pl.BlockSpec(memory_space=pltpu.VMEM)
    hbm = pl.BlockSpec(memory_space=pl.ANY)
    dma = pltpu.SemaphoreType.DMA
    return pl.pallas_call(
        functools.partial(kernel, n, num_tp),
        out_shape=jax.ShapeDtypeStruct((rows, half), jnp.bfloat16),
        in_specs=[vmem] * 5 + [hbm] * 3,
        out_specs=vmem,
        scratch_shapes=[
            pltpu.VMEM((n, rows, width), jnp.bfloat16),
            pltpu.VMEM((width, hidden), jnp.bfloat16),
            pltpu.VMEM((width, hidden), jnp.bfloat16),
            pltpu.VMEM((hidden, width), jnp.bfloat16),
            pltpu.VMEM((n, rows, half), jnp.float32),
            pltpu.VMEM((n, rows, half), jnp.bfloat16),
            pltpu.VMEM((n, rows, half), jnp.bfloat16),
            pltpu.VMEM((pairs, rows, half), jnp.bfloat16),
            pltpu.VMEM((pairs, rows, half), jnp.bfloat16),
            pltpu.VMEM((pairs, rows, half), jnp.bfloat16),
            pltpu.VMEM((pairs, rows, half), jnp.bfloat16),
            pltpu.VMEM((n, rows), jnp.float32),
            pltpu.VMEM((n, n, rows), jnp.float32),
            pltpu.VMEM((rows, LANES), jnp.float32),
            pltpu.VMEM((rows, LANES), jnp.float32),
            dma((3,)), dma((pairs,)), dma((pairs,)), dma((pairs,)), dma((pairs,)), dma((n,)), dma((n,)),
            dma((pairs,)), dma((pairs,)), dma((pairs,)), dma((pairs,)), dma((pairs,)), dma((pairs,)),
            dma((n,)), dma((n,)), dma, dma,
        ],
        compiler_params=pltpu.CompilerParams(collective_id=0, has_side_effects=True),
    )(tokens, routes.T, gate_weights.T, norm_gain.reshape(1, half), norm_bias.reshape(1, half),
      w_gate, w_up, w_down)


def solution(mesh):
    in_specs = (
        P(("grp", "ep"), None),
        P(("grp", "ep"), None),
        P(("grp", "ep"), None),
        P("ep", None, "tp"),
        P("ep", None, "tp"),
        P("ep", "tp", None),
        P("tp"),
        P("tp"),
    )
    out_specs = P(("grp", "ep"), "tp")
    body = functools.partial(shards, mesh.shape["ep"], mesh.shape["tp"])
    return jax.shard_map(body, mesh=mesh, in_specs=in_specs, out_specs=out_specs, check_vma=False)
```

time: 61.7 us -> 48.6 us (0.79)
  Pallas kernels: 57.2 us -> 46.9 us
  local copies, waits for them, and re-layouts: 4.32 us -> 1.57 us
    pallas_call x1, Pallas kernels: 57.2 us -> 46.9 us  [shards(): pl.pallas_call(functools.partial(kernel, n, num_tp), out_shape=jax.ShapeD...]
    unnamed x3 -> x1, local copies, waits for them, and re-layouts: 4.32 us -> 1.57 us
where the time goes in v2:
time: 48.6 us; the launch traced here: 48.5 us
  Pallas kernels  46.9 us (97%)
  local copies, waits for them, and re-layouts  1.57 us (3%)
    pallas_call x1, Pallas kernels, shards(): pl.pallas_call(functools.partial(kernel, n, num_tp), out_shape=jax.ShapeD...  46.9 us
    unnamed x1, local copies, waits for them, and re-layouts  1.57 us

profile of v2, /device:TPU:0, one launch (start us, length us, event | category | flops | bytes accessed | tf_op | source)
XLA Modules:
  0.0 48.5 jit_solution(2857290771981746930)
XLA Ops:
  0.0 46.9 %shard_map.82 = bf16[64,1024]{1,0:T(8,128)(2,1)} custom-call(bf16[64,2048]{1,0:T(8,128)(2,1)} %tokens.1, s32[4,64]{1,0:T(4,128)} %bitcast.6, f32[4,64]{1,0:T(4,128)} %bitcast.7, f32[1,1024]{1,0:T(1,128)} %bitcast.4, f32[1,1024]{1,0:T(1,128)} %bitcast.5, bf16[1,2048,640]{2,1,0:T(8,128)(2,1)} %wg_hbm.1, bf16[1,2048,640]{2,1,0:T(8,128)(2,1)} %wu_hbm.1, ...), custom_call_target="tpu_custom_call" | custom-call | tf_op jit(solution)/shard_map/pallas_call | solution.py:255
  46.9 1.6 %copy.10 = bf16[64,1024]{1,0:T(8,128)(2,1)} copy(bf16[64,1024]{1,0:T(8,128)(2,1)} %shard_map.82) | data formatting | bytes 262144

commit v3 on v2

--- a/solution.py
+++ b/solution.py
@@ -10,6 +10,7 @@
 norm_eps = 1e-05
 MESH = pl.DeviceIdType.MESH
 LANES = 128
+CHUNKS = 2
 
 
 def kernel(n, num_tp, tokens, routes, weights, gain, bias, wg_hbm, wu_hbm, wd_hbm, out,
@@ -25,7 +26,6 @@
     pairs = n // 2
     z, y = me // 2, lax.rem(me, 2)
     partner = 2 * z + 1 - y
-    my_rows = pl.ds(pl.multiple_of(core * share, share), share)
     my_cols = pl.ds(pl.multiple_of(core * half, half), half)
     other_cols = pl.ds(pl.multiple_of(other * half, half), half)
 
@@ -55,22 +55,30 @@
             bit *= 2
         return total
 
-    def own_copy():
-        return pltpu.make_async_remote_copy(
-            src_ref=tokens.at[my_rows, :], dst_ref=xs.at[me, my_rows, :],
-            send_sem=ys.at[z], recv_sem=yr.at[z],
+    def my_chunk(c):
+        chunk = share // CHUNKS
+        return pl.ds(pl.multiple_of(core * share + c * chunk, chunk), chunk)
+
+    def chunk_of(c):
+        chunk = rows // CHUNKS
+        return pl.ds(c * chunk, chunk)
+
+    def own_copy(c):
+        return pltpu.make_async_remote_copy(
+            src_ref=tokens.at[my_chunk(c), :], dst_ref=xs.at[me, my_chunk(c), :],
+            send_sem=ys.at[z, c], recv_sem=yr.at[z, c],
             device_id={"ep": partner}, device_id_type=MESH)
 
-    def gather_copy(there, source):
-        return pltpu.make_async_remote_copy(
-            src_ref=tokens.at[my_rows, :], dst_ref=xs.at[2 * source + y, my_rows, :],
-            send_sem=gs.at[there], recv_sem=gr.at[source],
+    def gather_copy(there, source, c):
+        return pltpu.make_async_remote_copy(
+            src_ref=tokens.at[my_chunk(c), :], dst_ref=xs.at[2 * source + y, my_chunk(c), :],
+            send_sem=gs.at[there, c], recv_sem=gr.at[source, c],
             device_id={"ep": 2 * there + y}, device_id_type=MESH)
 
-    def across_copy(zz, side):
-        return pltpu.make_async_remote_copy(
-            src_ref=xs.at[2 * zz + side, my_rows, :], dst_ref=xs.at[2 * zz + side, my_rows, :],
-            send_sem=ys.at[zz], recv_sem=yr.at[zz],
+    def across_copy(zz, side, c):
+        return pltpu.make_async_remote_copy(
+            src_ref=xs.at[2 * zz + side, my_chunk(c), :], dst_ref=xs.at[2 * zz + side, my_chunk(c), :],
+            send_sem=ys.at[zz, c], recv_sem=yr.at[zz, c],
             device_id={"ep": partner}, device_id_type=MESH)
 
     def forward_copy(source, who):
@@ -87,16 +95,16 @@
             send_sem=ps.at[zz], recv_sem=pr.at[zz],
             device_id={"tp": other}, device_id_type=MESH)
 
-    def back_copy(zz):
-        return pltpu.make_async_remote_copy(
-            src_ref=y_out.at[zz], dst_ref=y_in.at[zz],
-            send_sem=vs.at[zz], recv_sem=vr.at[zz],
+    def back_copy(zz, c):
+        return pltpu.make_async_remote_copy(
+            src_ref=y_out.at[zz, chunk_of(c), :], dst_ref=y_in.at[zz, chunk_of(c), :],
+            send_sem=vs.at[zz, c], recv_sem=vr.at[zz, c],
             device_id={"ep": partner}, device_id_type=MESH)
 
-    def return_copy(there, source):
-        return pltpu.make_async_remote_copy(
-            src_ref=ret_out.at[there], dst_ref=ret_in.at[source],
-            send_sem=rs.at[there], recv_sem=rr.at[source],
+    def return_copy(there, source, c):
+        return pltpu.make_async_remote_copy(
+            src_ref=ret_out.at[there, chunk_of(c), :], dst_ref=ret_in.at[source, chunk_of(c), :],
+            send_sem=rs.at[there, c], recv_sem=rr.at[source, c],
             device_id={"ep": 2 * there + y}, device_id_type=MESH)
 
     def table_copy(there, source):
@@ -105,9 +113,11 @@
             send_sem=ts.at[there], recv_sem=tr.at[source],
             device_id={"ep": there}, device_id_type=MESH)
 
-    own_copy().start()
+    for c in range(CHUNKS):
+        own_copy(c).start()
     for g in range(1, pairs):
-        gather_copy(mate(g), z).start()
+        for c in range(CHUNKS):
+            gather_copy(mate(g), z, c).start()
     for k in range(1, n):
         table_copy(lax.rem(me + k, n), me).start()
 
@@ -122,31 +132,33 @@
         @pl.when((i > 0) & (i < pairs))
         def _():
             zz = mate(i)
-            gather_copy(zz, zz).wait_recv()
-            across_copy(zz, y).start()
+            for c in range(CHUNKS):
+                gather_copy(zz, zz, c).wait_recv()
+                across_copy(zz, y, c).start()
             forward_copy(2 * zz + y, core).start()
 
         @pl.when((i > 0) & (i <= pairs))
         def _():
             zz = mate(i - 1)
-            across_copy(zz, 1 - y).wait_recv()
+            for c in range(CHUNKS):
+                across_copy(zz, 1 - y, c).wait_recv()
             forward_copy(2 * zz + 1 - y, core).start()
 
-        @pl.when(i == 2)
+        @pl.when(i == 1)
         def _():
             for load in loads:
                 load.wait()
             forward_copy(partner, other).wait_recv()
 
-        @pl.when((i > 2) & (i <= pairs + 1))
-        def _():
-            zz = mate(i - 2)
+        @pl.when((i > 1) & (i <= pairs))
+        def _():
+            zz = mate(i - 1)
             forward_copy(2 * zz, other).wait_recv()
             forward_copy(2 * zz + 1, other).wait_recv()
 
-        @pl.when((i > 1) & (i <= pairs + 1))
-        def _():
-            zz = mate(i - 2)
+        @pl.when((i > 0) & (i <= pairs))
+        def _():
+            zz = mate(i - 1)
             block = pl.ds(2 * zz, 2)
             x = xs[block].reshape(2 * rows, width)
             gate = jnp.dot(x, wg[...], preferred_element_type=jnp.float32)
@@ -158,48 +170,53 @@
             mine = jnp.dot(hidden, wd[:, my_cols], preferred_element_type=jnp.float32)
             own[block] = mine.reshape(2, rows, half)
 
-        @pl.when(i == 3)
+        @pl.when(i == 1)
         def _():
             table_copy(partner, partner).wait_recv()
 
-        @pl.when((i > 3) & (i <= pairs + 2))
-        def _():
-            zz = mate(i - 3)
+        @pl.when((i > 1) & (i <= pairs))
+        def _():
+            zz = mate(i - 1)
             table_copy(partner, 2 * zz).wait_recv()
             table_copy(partner, 2 * zz + 1).wait_recv()
 
-        @pl.when((i > 2) & (i <= pairs + 2))
-        def _():
-            zz = mate(i - 3)
+        @pl.when((i > 0) & (i <= pairs))
+        def _():
+            zz = mate(i - 1)
             partial_copy(zz).wait_recv()
             away = 2 * zz + 1 - y
             total = own[away] + part_in[away].astype(jnp.float32)
             y_out[zz] = (total * weight_of(away)).astype(jnp.bfloat16)
-            back_copy(zz).start()
+            for c in range(CHUNKS):
+                back_copy(zz, c).start()
             here = 2 * zz + y
             total = own[here] + part_in[here].astype(jnp.float32)
             own[here] = total * weight_of(here)
 
-        @pl.when(i > 3)
-        def _():
-            zz = mate(i - 4)
+        @pl.when(i == 2)
+        def _():
+            for c in range(CHUNKS):
+                back_copy(z, c).wait_recv()
+            own[me] = own[me] + y_in[z].astype(jnp.float32)
+
+        @pl.when(i > 2)
+        def _():
+            zz = mate(i - 2)
             here = 2 * zz + y
-            back_copy(zz).wait_recv()
-            total = own[here] + y_in[zz].astype(jnp.float32)
-            own[here] = total
-            ret_out[zz] = total.astype(jnp.bfloat16)
-
-        @pl.when(i > 4)
-        def _():
-            return_copy(mate(i - 4), z).start()
+            for c in range(CHUNKS):
+                back_copy(zz, c).wait_recv()
+                total = own[here, chunk_of(c), :] + y_in[zz, chunk_of(c), :].astype(jnp.float32)
+                ret_out[zz, chunk_of(c), :] = total.astype(jnp.bfloat16)
+                return_copy(zz, z, c).start()
 
         return carry
 
-    lax.fori_loop(0, pairs + 4, step, 0)
+    lax.fori_loop(1, pairs + 2, step, 0)
 
     def collect(g, total):
         zz = mate(g)
-        return_copy(zz, zz).wait_recv()
+        for c in range(CHUNKS):
+            return_copy(zz, zz, c).wait_recv()
         return total + ret_in[zz].astype(jnp.float32)
 
     mixture = own[me]
@@ -216,19 +233,21 @@
         device_id={"tp": other}, device_id_type=MESH)
     stats.start()
 
-    own_copy().wait_send()
+    for c in range(CHUNKS):
+        own_copy(c).wait_send()
+        back_copy(z, c).wait_send()
     forward_copy(partner, core).wait_send()
     partial_copy(z).wait_send()
-    back_copy(z).wait_send()
     table_copy(partner, me).wait_send()
 
     def drain(g, carry):
         zz = mate(g)
-        gather_copy(zz, z).wait_send()
-        across_copy(zz, y).wait_send()
         partial_copy(zz).wait_send()
-        back_copy(zz).wait_send()
-        return_copy(zz, z).wait_send()
+        for c in range(CHUNKS):
+            gather_copy(zz, z, c).wait_send()
+            across_copy(zz, y, c).wait_send()
+            back_copy(zz, c).wait_send()
+            return_copy(zz, z, c).wait_send()
         for j in range(2):
             forward_copy(2 * zz + j, core).wait_send()
             table_copy(2 * zz + j, me).wait_send()
@@ -252,6 +271,7 @@
     vmem = pl.BlockSpec(memory_space=pltpu.VMEM)
     hbm = pl.BlockSpec(memory_space=pl.ANY)
     dma = pltpu.SemaphoreType.DMA
+    hop = dma((pairs, CHUNKS))
     return pl.pallas_call(
         functools.partial(kernel, n, num_tp),
         out_shape=jax.ShapeDtypeStruct((rows, half), jnp.bfloat16),
@@ -273,8 +293,8 @@
             pltpu.VMEM((n, n, rows), jnp.float32),
             pltpu.VMEM((rows, LANES), jnp.float32),
             pltpu.VMEM((rows, LANES), jnp.float32),
-            dma((3,)), dma((pairs,)), dma((pairs,)), dma((pairs,)), dma((pairs,)), dma((n,)), dma((n,)),
-            dma((pairs,)), dma((pairs,)), dma((pairs,)), dma((pairs,)), dma((pairs,)), dma((pairs,)),
+            dma((3,)), hop, hop, hop, hop, dma((n,)), dma((n,)),
+            dma((pairs,)), dma((pairs,)), hop, hop, hop, hop,
             dma((n,)), dma((n,)), dma, dma,
         ],
         compiler_params=pltpu.CompilerParams(collective_id=0, has_side_effects=True),

time: 48.6 us -> 47.1 us (0.969)
  Pallas kernels: 46.9 us -> 45.3 us
    pallas_call x1, Pallas kernels: 46.9 us -> 45.3 us  [shards(): pl.pallas_call(functools.partial(kernel, n, num_tp), out_shape=jax.ShapeD...]
where the time goes in v3:
time: 47.1 us; the launch traced here: 46.9 us
  Pallas kernels  45.3 us (96%)
  local copies, waits for them, and re-layouts  1.57 us (3%)
    pallas_call x1, Pallas kernels, shards(): pl.pallas_call(functools.partial(kernel, n, num_tp), out_shape=jax.ShapeD...  45.3 us
    unnamed x1, local copies, waits for them, and re-layouts  1.57 us

profile of v3, /device:TPU:0, one launch (start us, length us, event | category | flops | bytes accessed | tf_op | source)
XLA Modules:
  0.0 46.9 jit_solution(8943880613731793307)
XLA Ops:
  0.0 45.3 %shard_map.82 = bf16[64,1024]{1,0:T(8,128)(2,1)} custom-call(bf16[64,2048]{1,0:T(8,128)(2,1)} %tokens.1, s32[4,64]{1,0:T(4,128)} %bitcast.6, f32[4,64]{1,0:T(4,128)} %bitcast.7, f32[1,1024]{1,0:T(1,128)} %bitcast.4, f32[1,1024]{1,0:T(1,128)} %bitcast.5, bf16[1,2048,640]{2,1,0:T(8,128)(2,1)} %wg_hbm.1, bf16[1,2048,640]{2,1,0:T(8,128)(2,1)} %wu_hbm.1, ...), custom_call_target="tpu_custom_call" | custom-call | tf_op jit(solution)/shard_map/pallas_call | solution.py:275
  45.3 1.6 %copy.10 = bf16[64,1024]{1,0:T(8,128)(2,1)} copy(bf16[64,1024]{1,0:T(8,128)(2,1)} %shard_map.82) | data formatting | bytes 262144
